TPU v7x, 32 devices: a whole 2x2x4 slice. The times are simulated.
32 devices in a mesh: fs: 4 (over y, x), tp: 8 (over z, core).
Axes of the slice: x: 2, y: 2, z: 4, core: 2. Of those that a mesh axis runs over, the one named last changes fastest.
Arguments:
- tokens: bfloat16 [2048, 2048], P('fs', 'tp'), may hold values from -6 to 6
- norm_gain: float32 [2048], P('fs'), may hold values from 0.1 to 1.9
- gate_train: float32 [2048, 8192], P('fs', 'tp'), may hold values from -0.125 to 0.125
- up_train: float32 [2048, 8192], P('fs', 'tp'), may hold values from -0.125 to 0.125
- down_train: float32 [8192, 2048], P('fs', 'tp'), may hold values from -0.0625 to 0.0625
Outputs:
- gate_serve: bfloat16 [2048, 8192], P(None, 'tp')
- up_serve: bfloat16 [2048, 8192], P(None, 'tp')
- down_serve: bfloat16 [8192, 2048], P('tp')
- layer_out: bfloat16 [2048, 2048], P(('fs', 'tp'))
All inputs are finite; a program needn't handle non-finite values.
Results may differ from a plain program's by a relative error of at most 0.024.
Values may be sent and summed in bfloat16 or wider, within the bound.
A program may use at most 64 MiB of HBM per device.

v0:
```python
import jax
import jax.numpy as jnp
from jax import lax
from jax.sharding import PartitionSpec as P

D = 2048
epsilon = 1e-06


def body(tokens, norm_gain, gate_train, up_train, down_train):
    gate_local = (norm_gain[:, None] * gate_train).astype(jnp.bfloat16)
    up_local = (norm_gain[:, None] * up_train).astype(jnp.bfloat16)
    down_local = down_train.astype(jnp.bfloat16)
    features = lax.all_gather(tokens, "tp", axis=1, tiled=True)
    wide = features.astype(jnp.float32)
    squares = jnp.sum(wide * wide, axis=1)
    gate_whole, up_whole = (
        lax.all_gather(gate_local, "fs", axis=0, tiled=True),
        lax.all_gather(up_local, "fs", axis=0, tiled=True),
    )
    gate_sum = jnp.dot(features, gate_whole, preferred_element_type=jnp.float32)
    up_sum = jnp.dot(features, up_whole, preferred_element_type=jnp.float32)
    down_rows = lax.all_gather(down_local, "fs", axis=0, tiled=True)
    down_whole = lax.all_to_all(down_rows, "tp", split_axis=0, concat_axis=1, tiled=True)
    scale = lax.rsqrt(squares / D + epsilon)[:, None]
    hidden = (jax.nn.silu(gate_sum * scale) * (up_sum * scale)).astype(jnp.bfloat16)
    mixed = lax.psum_scatter(
        jnp.dot(hidden, down_whole, preferred_element_type=jnp.float32).astype(jnp.bfloat16),
        "tp",
        scatter_dimension=0,
        tiled=True,
    )
    return (gate_whole, up_whole, down_whole, mixed)


def solution(mesh):
    return jax.shard_map(
        body,
        mesh=mesh,
        in_specs=(P("fs", "tp"), P("fs"), P("fs", "tp"), P("fs", "tp"), P("fs", "tp")),
        out_specs=(P(None, "tp"), P(None, "tp"), P("tp", None), P(("fs", "tp"), None)),
        check_vma=False,
    )
```

profile of v0, /device:TPU:0, one launch (start us, length us, event | category | flops | bytes accessed | tf_op | source)
XLA Modules:
  0.0 293.7 jit_solution(2137613969868247611)
XLA Ops:
  7.2 0.0 copy-start.2
  7.2 0.0 copy-start.3
  7.2 0.0 all-gather.9.cloned.1.call-start
  7.2 2.8 convert_element_type.20
  10.0 0.0 all-gather.9.cloned.1.call-update
  10.1 0.0 all-gather.11.cloned.1.call-start
  10.1 0.7 all-gather.11.cloned.1.call-update
  10.8 0.0 all-gather.5.cloned.1.call-start
  10.9 0.0 copy-done.2
  10.9 0.0 copy-done.3
  10.9 3.2 %multiply_convert_fusion = (bf16[512,1024]{1,0:T(8,128)(2,1)}, bf16[512,1024]{1,0:T(8,128)(2,1)}) fusion(f32[512,1024]{1,0:T(8,128)S(1)} %copy-done.2, f32[512]{0:T(512)S(1)} %copy-done.3, f32[512,1024]{1,0:T(8,128)} %param.7), kind=kLoop, calls=%fused_computation.9 | loop fusion | flops 2097152 | bytes 6293504 | tf_op jit(solution)/shard_map/convert_element_type | solution.py:12
  14.1 0.0 all-gather.5.cloned.1.call-update
  14.1 51.6 %all-gather.9.cloned.1.call-done = bf16[8192,256]{1,0:T(8,128)(2,1)} async-done(((bf16[2048,256]{1,0:T(8,128)(2,1)}), bf16[8192,256]{1,0:T(8,128)(2,1)}) %all-gather.9.cloned.1.call-update) | async-done | bytes 4194320 | tf_op jit(solution)/shard_map/all_gather | solution.py:23
  65.7 4.6 %all-to-all-start = ((bf16[8,1024,256]{2,1,0:T(8,128)(2,1)}), bf16[8,1024,256]{2,1,0:T(8,128)(2,1)}, u32[]{:S(2)}, u32[]{:S(2)}) async-start(bf16[8,1024,256]{2,1,0:T(8,128)(2,1)} %bitcast.32), calls=%async_computation | async-start | bytes 8388608 | tf_op jit(solution)/shard_map/all_to_all | solution.py:24
  70.3 0.0 all-gather.7.cloned.1.call-start
  70.4 0.5 all-gather.7.cloned.1.call-update
  70.9 0.0 reduce-scatter.2.cloned.1.call-start
  71.0 50.9 %all-gather.11.cloned.1.call-done = bf16[512,2048]{1,0:T(8,128)(2,1)} async-done(((bf16[512,256]{1,0:T(8,128)(2,1)}), bf16[512,2048]{1,0:T(8,128)(2,1)}) %all-gather.11.cloned.1.call-update) | async-done | bytes 2097168 | tf_op jit(solution)/shard_map/all_gather | solution.py:14
  121.8 0.0 copy-start.1
  121.8 2.2 multiply_reduce_fusion
  124.1 54.8 %all-gather.5.cloned.1.call-done = bf16[2048,1024]{1,0:T(8,128)(2,1)} async-done(((bf16[512,1024]{1,0:T(8,128)(2,1)}), bf16[2048,1024]{1,0:T(8,128)(2,1)}) %all-gather.5.cloned.1.call-update) | async-done | bytes 4194320 | tf_op jit(solution)/shard_map/all_gather | solution.py:18
  178.9 0.0 copy-done.1
  178.9 5.9 %fusion.5 = f32[1024,512]{1,0:T(8,128)} fusion(bf16[2048,1024]{1,0:T(8,128)(2,1)} %all-gather.5.cloned.1.call-done, bf16[512,2048]{1,0:T(8,128)(2,1)S(1)} %copy-done.1), kind=kOutput, calls=%fused_computation.13 | convolution fusion | flops 2147483648 | bytes 8388608 | tf_op jit(solution)/shard_map/dot_general | solution.py:21
  184.8 0.0 all-to-all-done
  184.8 6.5 %copy.10 = bf16[8,1024,256]{1,2,0:T(8,128)(2,1)} copy(bf16[8,1024,256]{2,1,0:T(8,128)(2,1)} %all-to-all-done) | data formatting | bytes 8388608 | tf_op jit(solution)/shard_map/all_to_all | solution.py:24
  191.2 42.5 %all-gather.7.cloned.1.call-done = bf16[2048,1024]{1,0:T(8,128)(2,1)} async-done(((bf16[512,1024]{1,0:T(8,128)(2,1)}), bf16[2048,1024]{1,0:T(8,128)(2,1)}) %all-gather.7.cloned.1.call-update) | async-done | bytes 4194320 | tf_op jit(solution)/shard_map/all_gather | solution.py:19
  233.7 10.3 %convolution_convert_fusion = bf16[512,2048]{1,0:T(8,128)(2,1)} fusion(bf16[1024,2048]{0,1:T(8,128)(2,1)} %bitcast.30, f32[1024,512]{1,0:T(8,128)} %fusion.5, bf16[2048,1024]{1,0:T(8,128)(2,1)} %all-gather.7.cloned.1.call-done, bf16[512,2048]{1,0:T(8,128)(2,1)S(1)} %copy-done.1, f32[512]{0:T(512)S(1)} %add_rsqrt_fusion), kind=kOutput, calls=%fused_computation.1 | convolution fusion | flops 4300210176 | bytes 14682112 | tf_op jit(solution)/shard_map/dot_general | solution.py:28
  244.0 0.0 reduce-scatter.2.cloned.1.call-update
  244.0 6.4 %copy.11 = bf16[1024,2048]{1,0:T(8,128)(2,1)} copy(bf16[1024,2048]{0,1:T(8,128)(2,1)} %bitcast.31) | data formatting | bytes 8388608
  250.5 29.8 %reduce-scatter.2.cloned.1.call-done = bf16[64,2048]{1,0:T(8,128)(2,1)} async-done(((bf16[512,2048]{1,0:T(8,128)(2,1)}), bf16[64,2048]{1,0:T(8,128)(2,1)}) %reduce-scatter.2.cloned.1.call-update) | async-done | bytes 262160 | tf_op jit(solution)/shard_map/reduce_scatter | solution.py:27
  280.3 0.0 copy-start
  280.3 4.8 %copy.14 = bf16[2048,1024]{1,0:T(8,128)(2,1)} copy(bf16[2048,1024]{1,0:T(8,128)(2,1)} %all-gather.5.cloned.1.call-done) | data formatting | bytes 8388608
  285.1 0.0 copy-done
  285.1 2.0 copy.15
  (1 shorter events, 0.0 us)
Async XLA Ops:
  7.2 3.7 %copy-start.2 = (f32[512,1024]{1,0:T(8,128)S(1)}, f32[512,1024]{1,0:T(8,128)}, u32[]{:S(2)}) copy-start(f32[512,1024]{1,0:T(8,128)} %param.8) | copy-start | bytes 6291460
  7.2 3.7 %copy-start.3 = (f32[512]{0:T(512)S(1)}, f32[512]{0:T(512)}, u32[]{:S(2)}) copy-start(f32[512]{0:T(512)} %param.6) | copy-start | bytes 6148
  7.2 58.6 %all-gather.9.cloned.1.call-start = ((), (), s32[]{:S(2)}) async-start(), calls=%async_computation.4 | async-start | bytes 5242880 | tf_op jit(solution)/shard_map/all_gather | solution.py:23
  10.1 111.8 %all-gather.11.cloned.1.call-start = ((), (), s32[]{:S(2)}) async-start(), calls=%async_computation.5 | async-start | bytes 2359296 | tf_op jit(solution)/shard_map/all_gather | solution.py:14
  10.8 168.1 %all-gather.5.cloned.1.call-start = ((), (), s32[]{:S(2)}) async-start(), calls=%async_computation.2 | async-start | bytes 5242880 | tf_op jit(solution)/shard_map/all_gather | solution.py:18
  65.7 119.0 %all-to-all-start = ((bf16[8,1024,256]{2,1,0:T(8,128)(2,1)}), bf16[8,1024,256]{2,1,0:T(8,128)(2,1)}, u32[]{:S(2)}, u32[]{:S(2)}) async-start(bf16[8,1024,256]{2,1,0:T(8,128)(2,1)} %bitcast.32), calls=%async_computation | async-start | bytes 8388608 | tf_op jit(solution)/shard_map/all_to_all | solution.py:24
  70.3 163.4 %all-gather.7.cloned.1.call-start = ((), (), s32[]{:S(2)}) async-start(), calls=%async_computation.3 | async-start | bytes 5242880 | tf_op jit(solution)/shard_map/all_gather | solution.py:19
  70.9 209.4 %reduce-scatter.2.cloned.1.call-start = ((), (), s32[]{:S(2)}) async-start(), calls=%async_computation.6 | async-start | bytes 2359296 | tf_op jit(solution)/shard_map/reduce_scatter | solution.py:27
  121.8 57.0 %copy-start.1 = (bf16[512,2048]{1,0:T(8,128)(2,1)S(1)}, bf16[512,2048]{1,0:T(8,128)(2,1)}, u32[]{:S(2)}) copy-start(bf16[512,2048]{1,0:T(8,128)(2,1)} %all-gather.11.cloned.1.call-done) | copy-start | bytes 6291460
  280.3 4.8 %copy-start = (bf16[2048,1024]{1,0:T(8,128)(2,1)S(1)}, bf16[2048,1024]{1,0:T(8,128)(2,1)}, u32[]{:S(2)}) copy-start(bf16[2048,1024]{1,0:T(8,128)(2,1)} %all-gather.7.cloned.1.call-done) | copy-start | bytes 12582916
Sparse Core Ops, SparseCore 0:
  10.4 55.2 all-gather.8
  67.3 54.4 all-gather.10
  124.3 54.5 all-gather.4
  181.1 52.5 all-gather.6
  244.2 36.0 reduce-scatter.1
where the time goes:
time: 294 us
  waiting for transfers between devices  231 us (79%)
  local copies, waits for them, and re-layouts  19.8 us (7%)
  matrix products  16.2 us (6%)
  between operations  13.8 us (5%)
  other arithmetic  8.23 us (3%)
  starting transfers between devices  4.8 us (2%)
    all_gather x1, waiting for transfers between devices, body(): lax.all_gather(gate_local, 'fs', axis=0, tiled=True)  54.8 us
    all_gather x1, waiting for transfers between devices, body(): down_rows = lax.all_gather(down_local, 'fs', axis=0, tiled=True)  51.6 us
    all_gather x1, waiting for transfers between devices, body(): features = lax.all_gather(tokens, 'tp', axis=1, tiled=True)  50.9 us
    all_gather x1, waiting for transfers between devices, body(): lax.all_gather(up_local, 'fs', axis=0, tiled=True)  42.5 us
    reduce_scatter x1, waiting for transfers between devices, body(): lax.psum_scatter(jnp.dot(hidden, down_whole, preferred_element_type=jnp.f...  29.8 us
    unnamed x11, local copies, waits for them, and re-layouts  13.3 us
    dot_general x1, matrix products, body(): jnp.dot(hidden, down_whole, preferred_element_type=jnp.float32)  10.3 us
    all_to_all x1, local copies, waits for them, and re-layouts, body(): lax.all_to_all(down_rows, 'tp', split_axis=0, concat_axis=1, tiled=True)  6.48 us
  transfers between devices with their start and end apart: 6, of which 5 were waited for; matrix products, arithmetic and copies ran while one was open for 8% of the time, Pallas kernels for 0%

commit v1 on v0

--- a/solution.py
+++ b/solution.py
@@ -5,6 +5,19 @@
 
 D = 2048
 epsilon = 1e-06
+
+
+def gather_around(x, axis, dim):
+    ways = lax.axis_size(axis)
+    up = [(d, (d + 1) % ways) for d in range(ways)]
+    down = [(d, (d - 1) % ways) for d in range(ways)]
+    earlier, later = ([x], [x])
+    for _ in range(ways // 2):
+        earlier.append(lax.ppermute(earlier[-1], axis, up))
+    for _ in range((ways - 1) // 2):
+        later.append(lax.ppermute(later[-1], axis, down))
+    line = jnp.concatenate([*earlier[::-1], *later[1:]], axis=dim)
+    return jnp.roll(line, (lax.axis_index(axis) - ways // 2) * x.shape[dim], axis=dim)
 
 
 def body(tokens, norm_gain, gate_train, up_train, down_train):
@@ -16,7 +29,7 @@
     squares = jnp.sum(wide * wide, axis=1)
     gate_whole, up_whole = (
         lax.all_gather(gate_local, "fs", axis=0, tiled=True),
-        lax.all_gather(up_local, "fs", axis=0, tiled=True),
+        gather_around(up_local, "fs", 0),
     )
     gate_sum = jnp.dot(features, gate_whole, preferred_element_type=jnp.float32)
     up_sum = jnp.dot(features, up_whole, preferred_element_type=jnp.float32)

time: 294 us -> 260 us (0.88)
  waiting for transfers between devices: 231 us -> 188 us
  starting transfers between devices: 4.8 us -> 9.34 us
  local copies, waits for them, and re-layouts: 19.8 us -> 23.1 us
    ppermute x0 -> x3, waiting for transfers between devices: none -> 79.9 us  [the longest x2 49.1 us: gather_around(): earlier.append(lax.ppermute(earlier[-1], axis, up))]
    all_gather x1, waiting for transfers between devices: 50.9 us -> 0.01 us  [body(): features = lax.all_gather(tokens, 'tp', axis=1, tiled=True)]
    all_gather x1 -> x0, waiting for transfers between devices: 42.5 us -> none  [body(): lax.all_gather(up_local, 'fs', axis=0, tiled=True)]
    all_gather x1, waiting for transfers between devices: 54.8 us -> 22.7 us  [body(): lax.all_gather(gate_local, 'fs', axis=0, tiled=True)]
    ppermute x0 -> x3, starting transfers between devices: none -> 4.45 us  [the longest x1 2.36 us: gather_around(): later.append(lax.ppermute(later[-1], axis, down))]
    all_gather x1, waiting for transfers between devices: 51.6 us -> 55.1 us  [body(): down_rows = lax.all_gather(down_local, 'fs', axis=0, tiled=True)]
    unnamed x11 -> x15, local copies, waits for them, and re-layouts: 13.3 us -> 14 us
  transfers between devices with their start and end apart: 6 -> 8, of which waited for: 5 -> 6; matrix products, arithmetic and copies ran while one was open for 8% -> 9% of each run, Pallas kernels for 0% -> 0%
where the time goes in v1:
time: 260 us
  waiting for transfers between devices  188 us (72%)
  local copies, waits for them, and re-layouts  23.1 us (9%)
  matrix products  16.9 us (6%)
  between operations  13.8 us (5%)
  starting transfers between devices  9.34 us (4%)
  other arithmetic  8.21 us (3%)
    all_gather x1, waiting for transfers between devices, body(): down_rows = lax.all_gather(down_local, 'fs', axis=0, tiled=True)  55.1 us
    ppermute x2, waiting for transfers between devices, gather_around(): earlier.append(lax.ppermute(earlier[-1], axis, up))  49.1 us
    ppermute x1, waiting for transfers between devices, gather_around(): later.append(lax.ppermute(later[-1], axis, down))  30.9 us
    reduce_scatter x1, waiting for transfers between devices, body(): lax.psum_scatter(jnp.dot(hidden, down_whole, preferred_element_type=jnp.f...  29.7 us
    all_gather x1, waiting for transfers between devices, body(): lax.all_gather(gate_local, 'fs', axis=0, tiled=True)  22.7 us
    unnamed x15, local copies, waits for them, and re-layouts  14 us
    dot_general x1, matrix products, body(): jnp.dot(hidden, down_whole, preferred_element_type=jnp.float32)  10.3 us
    all_to_all x1, local copies, waits for them, and re-layouts, body(): lax.all_to_all(down_rows, 'tp', split_axis=0, concat_axis=1, tiled=True)  6.58 us
  transfers between devices with their start and end apart: 8, of which 6 were waited for; matrix products, arithmetic and copies ran while one was open for 9% of the time, Pallas kernels for 0%

profile of v1, /device:TPU:0, one launch (start us, length us, event | category | flops | bytes accessed | tf_op | source)
XLA Modules:
  0.0 259.5 jit_solution(3246727897130950576)
XLA Ops:
  7.2 0.0 all-gather.6.cloned.1.call-start
  7.2 2.7 %convert_element_type.20 = bf16[2048,256]{1,0:T(8,128)(2,1)} convert(f32[2048,256]{1,0:T(8,128)} %param.9) | non-fusion elementwise | flops 524288 | bytes 3145728 | tf_op jit(solution)/shard_map/convert_element_type | solution.py:26
  9.9 0.0 all-gather.6.cloned.1.call-update
  9.9 0.0 all-gather.8.cloned.1.call-start
  9.9 0.7 all-gather.8.cloned.1.call-update
  10.7 55.1 %all-gather.6.cloned.1.call-done = bf16[8192,256]{1,0:T(8,128)(2,1)} async-done(((bf16[2048,256]{1,0:T(8,128)(2,1)}), bf16[8192,256]{1,0:T(8,128)(2,1)}) %all-gather.6.cloned.1.call-update) | async-done | bytes 4194320 | tf_op jit(solution)/shard_map/all_gather | solution.py:36
  65.7 0.0 copy-start.1
  65.7 0.0 copy-start.2
  65.7 4.7 %all-to-all-start = ((bf16[8,1024,256]{2,1,0:T(8,128)(2,1)}), bf16[8,1024,256]{2,1,0:T(8,128)(2,1)}, u32[]{:S(2)}, u32[]{:S(2)}) async-start(bf16[8,1024,256]{2,1,0:T(8,128)(2,1)} %bitcast.32), calls=%async_computation | async-start | bytes 8388608 | tf_op jit(solution)/shard_map/all_to_all | solution.py:37
  70.5 0.0 all-gather.4.cloned.1.call-start
  70.5 0.0 copy-done.1
  70.5 0.0 copy-done.2
  70.5 2.9 %multiply_convert_fusion = (bf16[512,1024]{1,0:T(8,128)(2,1)S(1)}, bf16[512,1024]{1,0:T(8,128)(2,1)}) fusion(f32[512,1024]{1,0:T(8,128)S(1)} %copy-done.1, f32[512]{0:T(512)S(1)} %copy-done.2, f32[512,1024]{1,0:T(8,128)} %param.7), kind=kLoop, calls=%fused_computation.9 | loop fusion | flops 2097152 | bytes 6293504 | tf_op jit(solution)/shard_map/convert_element_type | solution.py:25
  73.4 0.0 all-gather.4.cloned.1.call-update
  73.4 0.0 reduce-scatter.2.cloned.1.call-start
  73.5 1.5 collective-permute-start
  75.0 25.0 %collective-permute-done = bf16[512,1024]{1,0:T(8,128)(2,1)S(1)} collective-permute-done((bf16[512,1024]{1,0:T(8,128)(2,1)S(1)}, bf16[512,1024]{1,0:T(8,128)(2,1)S(1)}, u32[]{:S(2)}, u32[]{:S(2)}) %collective-permute-start) | collective-permute-done | bytes 1048608 | tf_op jit(solution)/shard_map/ppermute | solution.py:16
  99.9 0.6 collective-permute-start.1
  100.5 2.4 collective-permute-start.2
  102.9 24.1 %collective-permute-done.1 = bf16[512,1024]{1,0:T(8,128)(2,1)} collective-permute-done((bf16[512,1024]{1,0:T(8,128)(2,1)S(1)}, bf16[512,1024]{1,0:T(8,128)(2,1)}, u32[]{:S(2)}, u32[]{:S(2)}) %collective-permute-start.1) | collective-permute-done | bytes 1048608 | tf_op jit(solution)/shard_map/ppermute | solution.py:16
  127.0 1.3 constant_dynamic-update-slice_fusion.7
  128.3 0.1 constant_dynamic-update-slice_fusion.6
  128.3 0.1 constant_dynamic-update-slice_fusion.5
  128.4 30.9 %collective-permute-done.2 = bf16[512,1024]{1,0:T(8,128)(2,1)S(1)} collective-permute-done((bf16[512,1024]{1,0:T(8,128)(2,1)S(1)}, bf16[512,1024]{1,0:T(8,128)(2,1)S(1)}, u32[]{:S(2)}, u32[]{:S(2)}) %collective-permute-start.2) | collective-permute-done | bytes 1048608 | tf_op jit(solution)/shard_map/ppermute | solution.py:18
  159.3 0.1 constant_dynamic-update-slice_fusion.4
  159.4 1.3 constant_dynamic-update-slice_fusion.3
  160.7 0.1 constant_dynamic-update-slice_fusion.2
  160.8 0.1 constant_dynamic-update-slice_fusion.1
  160.8 0.1 constant_dynamic-update-slice_fusion
  160.9 2.5 constant_dynamic-slice_fusion
  163.4 0.0 all-gather.8.cloned.1.call-done
  163.4 2.7 %multiply_reduce_fusion = f32[512]{0:T(512)S(1)} fusion(bf16[512,2048]{1,0:T(8,128)(2,1)} %all-gather.8.cloned.1.call-done), kind=kLoop, calls=%fused_computation | loop fusion | flops 3145216 | bytes 2099200 | tf_op jit(solution)/shard_map/reduce_sum | solution.py:29
  166.1 22.7 %all-gather.4.cloned.1.call-done = bf16[2048,1024]{1,0:T(8,128)(2,1)} async-done(((bf16[512,1024]{1,0:T(8,128)(2,1)}), bf16[2048,1024]{1,0:T(8,128)(2,1)}) %all-gather.4.cloned.1.call-update) | async-done | bytes 4194320 | tf_op jit(solution)/shard_map/all_gather | solution.py:31
  188.8 6.6 %fusion.5 = f32[1024,512]{1,0:T(8,128)} fusion(bf16[2048,1024]{1,0:T(8,128)(2,1)} %all-gather.4.cloned.1.call-done, bf16[512,2048]{1,0:T(8,128)(2,1)} %all-gather.8.cloned.1.call-done), kind=kOutput, calls=%fused_computation.22 | convolution fusion | flops 2147483648 | bytes 8388608 | tf_op jit(solution)/shard_map/dot_general | solution.py:34
  195.3 0.0 copy-start
  195.3 0.0 all-to-all-done
  195.3 6.6 %copy.10 = bf16[8,1024,256]{1,2,0:T(8,128)(2,1)} copy(bf16[8,1024,256]{2,1,0:T(8,128)(2,1)} %all-to-all-done) | data formatting | bytes 8388608 | tf_op jit(solution)/shard_map/all_to_all | solution.py:37
  201.9 0.0 copy-done
  201.9 10.3 %convolution_convert_fusion = bf16[512,2048]{1,0:T(8,128)(2,1)} fusion(bf16[1024,2048]{0,1:T(8,128)(2,1)} %bitcast.30, f32[1024,512]{1,0:T(8,128)} %fusion.5, bf16[2048,1024]{1,0:T(8,128)(2,1)} %constant_dynamic-slice_fusion, bf16[512,2048]{1,0:T(8,128)(2,1)S(1)} %copy-done, f32[512]{0:T(512)S(1)} %add_rsqrt_fusion), kind=kOutput, calls=%fused_computation.1 | convolution fusion | flops 4300210176 | bytes 14682112 | tf_op jit(solution)/shard_map/dot_general | solution.py:41
  212.2 0.0 reduce-scatter.2.cloned.1.call-update
  212.2 6.4 %copy.11 = bf16[1024,2048]{1,0:T(8,128)(2,1)} copy(bf16[1024,2048]{0,1:T(8,128)(2,1)} %bitcast.31) | data formatting | bytes 8388608
  218.7 29.7 %reduce-scatter.2.cloned.1.call-done = bf16[64,2048]{1,0:T(8,128)(2,1)} async-done(((bf16[512,2048]{1,0:T(8,128)(2,1)}), bf16[64,2048]{1,0:T(8,128)(2,1)}) %reduce-scatter.2.cloned.1.call-update) | async-done | bytes 262160 | tf_op jit(solution)/shard_map/reduce_scatter | solution.py:40
  248.3 4.6 %copy.20 = bf16[2048,1024]{1,0:T(8,128)(2,1)} copy(bf16[2048,1024]{1,0:T(8,128)(2,1)} %all-gather.4.cloned.1.call-done) | data formatting | bytes 8388608
  (1 shorter events, 0.0 us)
Async XLA Ops:
  7.2 58.6 %all-gather.6.cloned.1.call-start = ((), (), s32[]{:S(2)}) async-start(), calls=%async_computation.3 | async-start | bytes 5242880 | tf_op jit(solution)/shard_map/all_gather | solution.py:36
  9.9 153.5 %all-gather.8.cloned.1.call-start = ((), (), s32[]{:S(2)}) async-start(), calls=%async_computation.4 | async-start | bytes 2359296 | tf_op jit(solution)/shard_map/all_gather | solution.py:27
  65.7 4.8 %copy-start.1 = (f32[512,1024]{1,0:T(8,128)S(1)}, f32[512,1024]{1,0:T(8,128)}, u32[]{:S(2)}) copy-start(f32[512,1024]{1,0:T(8,128)} %param.8) | copy-start | bytes 6291460
  65.7 4.8 %copy-start.2 = (f32[512]{0:T(512)S(1)}, f32[512]{0:T(512)}, u32[]{:S(2)}) copy-start(f32[512]{0:T(512)} %param.6) | copy-start | bytes 6148
  65.7 129.6 %all-to-all-start = ((bf16[8,1024,256]{2,1,0:T(8,128)(2,1)}), bf16[8,1024,256]{2,1,0:T(8,128)(2,1)}, u32[]{:S(2)}, u32[]{:S(2)}) async-start(bf16[8,1024,256]{2,1,0:T(8,128)(2,1)} %bitcast.32), calls=%async_computation | async-start | bytes 8388608 | tf_op jit(solution)/shard_map/all_to_all | solution.py:37
  70.5 118.3 %all-gather.4.cloned.1.call-start = ((), (), s32[]{:S(2)}) async-start(), calls=%async_computation.2 | async-start | bytes 5242880 | tf_op jit(solution)/shard_map/all_gather | solution.py:31
  73.4 174.9 %reduce-scatter.2.cloned.1.call-start = ((), (), s32[]{:S(2)}) async-start(), calls=%async_computation.5 | async-start | bytes 2359296 | tf_op jit(solution)/shard_map/reduce_scatter | solution.py:40
  73.5 26.5 %collective-permute-start = (bf16[512,1024]{1,0:T(8,128)(2,1)S(1)}, bf16[512,1024]{1,0:T(8,128)(2,1)S(1)}, u32[]{:S(2)}, u32[]{:S(2)}) collective-permute-start(bf16[512,1024]{1,0:T(8,128)(2,1)S(1)} %get-tuple-element.8), channel_id=1, source_target_pairs={{0,8},{8,16},{16,24},{24,0},{1,9},{9,17},{17,25},{25,1},{2,10},{10... | collective-permute-start | bytes 3145736 | tf_op jit(solution)/shard_map/ppermute | solution.py:16
  99.9 27.0 %collective-permute-start.1 = (bf16[512,1024]{1,0:T(8,128)(2,1)S(1)}, bf16[512,1024]{1,0:T(8,128)(2,1)}, u32[]{:S(2)}, u32[]{:S(2)}) collective-permute-start(bf16[512,1024]{1,0:T(8,128)(2,1)S(1)} %collective-permute-done), channel_id=1, source_target_pairs={{0,8},{8,16},{16,24},{24,0},{1,9},{9,17},{17,25},{25,1},{2,10},{10... | collective-permute-start | bytes 3145736 | tf_op jit(solution)/shard_map/ppermute | solution.py:16
  100.5 58.8 %collective-permute-start.2 = (bf16[512,1024]{1,0:T(8,128)(2,1)S(1)}, bf16[512,1024]{1,0:T(8,128)(2,1)S(1)}, u32[]{:S(2)}, u32[]{:S(2)}) collective-permute-start(bf16[512,1024]{1,0:T(8,128)(2,1)S(1)} %get-tuple-element.8), channel_id=1, source_target_pairs={{0,24},{8,0},{16,8},{24,16},{1,25},{9,1},{17,9},{25,17},{2,26},{10... | collective-permute-start | bytes 3145736 | tf_op jit(solution)/shard_map/ppermute | solution.py:18
  195.3 6.6 %copy-start = (bf16[512,2048]{1,0:T(8,128)(2,1)S(1)}, bf16[512,2048]{1,0:T(8,128)(2,1)}, u32[]{:S(2)}) copy-start(bf16[512,2048]{1,0:T(8,128)(2,1)} %all-gather.8.cloned.1.call-done) | copy-start | bytes 6291460
Sparse Core Ops, SparseCore 0:
  10.4 55.2 all-gather.5
  67.3 54.5 all-gather.7
  124.3 64.3 all-gather.3
  212.4 35.9 reduce-scatter.1
